TPU v7x, 32 devices: a whole 2x2x4 slice. The times are simulated.
32 devices in a mesh: grp: 2 (over y), fs: 4 (over z), tp: 4 (over x, core).
Axes of the slice: x: 2, y: 2, z: 4, core: 2. Of those that a mesh axis runs over, the one named last changes fastest.
Arguments:
- stream: bfloat16 [2048, 3072], P('tp', ('grp', 'fs')), parts along dimension 1, may hold values from -6 to 6
- mixer_gain: float32 [2048], replicated, may hold values from 0.1 to 1.9
- glu_value: bfloat16 [2048, 1024], P('fs', 'tp'), may hold values from -0.125 to 0.125
- glu_gate: bfloat16 [2048, 1024], P('fs', 'tp'), may hold values from -0.125 to 0.125
- conv_kernel: bfloat16 [31, 1024], replicated, may hold values from -1 to 1
- channel_gain: float32 [1024], replicated, may hold values from 0.1 to 1.9
- conv_out: bfloat16 [2048, 1024], P('fs', 'tp'), may hold values from -0.1875 to 0.1875
- ffn_gain: float32 [2048], replicated, may hold values from 0.1 to 1.9
- ffn_gate: bfloat16 [2048, 5632], P('fs', 'tp'), may hold values from -0.125 to 0.125
- ffn_up: bfloat16 [2048, 5632], P('fs', 'tp'), may hold values from -0.125 to 0.125
- ffn_down: bfloat16 [2048, 5632], P('fs', 'tp'), may hold values from -0.078125 to 0.078125
Outputs:
- result: bfloat16 [2048, 3072], P('tp', ('grp', 'fs')), parts along dimension 1
There are 2 independent parts, one for each index of `grp`. A program takes and returns all parts, laid end to end along the dimension named above; an argument that names none is the same for every part. Nothing has to cross between parts.
All inputs are finite; a program needn't handle non-finite values.
Results may differ from a plain program's by a relative error of at most 0.018.
Values may be sent and summed in bfloat16 or wider, within the bound.
A program may use at most 64 MiB of HBM per device.

v0:
```python
import jax
import jax.numpy as jnp
from jax import lax
from jax.sharding import PartitionSpec as P


def rms_normalize(wide, gain):
    inverse = lax.rsqrt(jnp.mean(wide * wide, axis=0, keepdims=True) + 1e-06)
    return (wide * inverse * gain[:, None]).astype(jnp.bfloat16)


def contract(weight, acts):
    return lax.dot_general(
        weight, acts, (((0,), (0,)), ((), ())), preferred_element_type=jnp.float32
    )


def on_device(
    stream,
    mixer_gain,
    glu_value,
    glu_gate,
    conv_kernel,
    channel_gain,
    conv_out,
    ffn_gain,
    ffn_gate,
    ffn_up,
    ffn_down,
):
    length = stream.shape[1]
    channels = glu_value.shape[1]
    position = lax.axis_index("tp")
    total_channels = channels * lax.axis_size("tp")
    taps = lax.dynamic_slice_in_dim(conv_kernel, position * channels, channels, 1).astype(
        jnp.float32
    )
    gain_local = lax.dynamic_slice_in_dim(channel_gain, position * channels, channels, 0)
    gathered = lax.all_gather(stream, "tp", axis=0, tiled=True)
    normed = rms_normalize(gathered.astype(jnp.float32), mixer_gain)
    value_w, gate_w, out_w = (
        lax.all_gather(glu_value, "fs", axis=0, tiled=True),
        lax.all_gather(glu_gate, "fs", axis=0, tiled=True),
        lax.all_gather(conv_out, "fs", axis=0, tiled=True),
    )
    value_part = contract(value_w, normed)
    gate_part = contract(gate_w, normed)
    gated = (value_part * jax.nn.sigmoid(gate_part)).astype(jnp.bfloat16).astype(jnp.float32)
    padded = jnp.pad(gated, ((0, 0), (taps.shape[0] - 1, 0)))
    conv_sum = jnp.zeros_like(gated)
    for step in range(taps.shape[0]):
        conv_sum = conv_sum + taps[step][:, None] * padded[:, step : step + length]
    sums, squares = lax.psum(
        (jnp.sum(conv_sum, axis=0), jnp.sum(conv_sum * conv_sum, axis=0)), "tp"
    )
    mean_val = sums / total_channels
    mean_sq = squares / total_channels
    scaled = (
        (conv_sum - mean_val[None, :])
        * lax.rsqrt(mean_sq - mean_val * mean_val + 1e-05)[None, :]
        * gain_local[:, None]
    )
    activated = jax.nn.silu(scaled).astype(jnp.bfloat16)
    mixed_sum = lax.psum_scatter(
        jnp.dot(out_w, activated, preferred_element_type=jnp.float32).astype(jnp.bfloat16),
        "tp",
        scatter_dimension=0,
        tiled=True,
    ).astype(jnp.float32)
    middle_wide = stream.astype(jnp.float32) + mixed_sum
    middle = middle_wide.astype(jnp.bfloat16)
    gathered_two = lax.all_gather(middle, "tp", axis=0, tiled=True)
    normed_two = rms_normalize(gathered_two.astype(jnp.float32), ffn_gain)
    gate_whole, up_whole = (
        lax.all_gather(ffn_gate, "fs", axis=0, tiled=True),
        lax.all_gather(ffn_up, "fs", axis=0, tiled=True),
    )
    gate_val = contract(gate_whole, normed_two)
    up_val = contract(up_whole, normed_two)
    hidden = (jax.nn.silu(gate_val) * up_val).astype(jnp.bfloat16)
    down_whole = lax.all_gather(ffn_down, "fs", axis=0, tiled=True)
    ffn_sum = lax.psum_scatter(
        jnp.dot(down_whole, hidden, preferred_element_type=jnp.float32).astype(jnp.bfloat16),
        "tp",
        scatter_dimension=0,
        tiled=True,
    ).astype(jnp.float32)
    return (middle.astype(jnp.float32) + ffn_sum).astype(jnp.bfloat16)


def solution(mesh):
    in_specs = (
        P("tp", ("grp", "fs")),
        P(),
        P("fs", "tp"),
        P("fs", "tp"),
        P(),
        P(),
        P("fs", "tp"),
        P(),
        P("fs", "tp"),
        P("fs", "tp"),
        P("fs", "tp"),
    )
    out_specs = P("tp", ("grp", "fs"))
    return jax.shard_map(
        on_device, mesh=mesh, in_specs=in_specs, out_specs=out_specs, check_vma=False
    )
```

profile of v0, /device:TPU:0, one launch (start us, length us, event | category | flops | bytes accessed | tf_op | source)
XLA Modules:
  0.0 538.9 jit_solution(6192163965069522078)
XLA Ops:
  6.5 0.0 copy-start.4
  6.5 0.0 all-gather.9.cloned.1.call-start
  6.5 0.7 all-gather.9.cloned.1.call-update
  7.3 0.0 all-gather.13.cloned.1.call-start
  7.3 0.7 all-gather.13.cloned.1.call-update
  8.0 0.0 all-gather.11.cloned.1.call-start
  8.1 0.7 all-gather.11.cloned.1.call-update
  8.7 0.0 all-gather.15.cloned.1.call-start
  8.8 0.5 all-gather.15.cloned.1.call-update
  9.3 0.0 reduce-scatter.3.cloned.1.call-start
  9.4 0.7 dynamic-slice_convert_fusion
  10.1 0.8 dynamic_slice.7
  10.9 20.4 %all-gather.9.cloned.1.call-done = bf16[2048,384]{1,0:T(8,128)(2,1)} async-done(((bf16[512,384]{1,0:T(8,128)(2,1)}), bf16[2048,384]{1,0:T(8,128)(2,1)}) %all-gather.9.cloned.1.call-update) | async-done | bytes 1572880 | tf_op jit(solution)/shard_map/all_gather | solution.py:39
  31.3 1.8 fusion
  33.1 0.0 copy-start.1
  33.1 27.8 %all-gather.13.cloned.1.call-done = bf16[2048,256]{1,0:T(8,128)(2,1)} async-done(((bf16[512,256]{1,0:T(8,128)(2,1)}), bf16[2048,256]{1,0:T(8,128)(2,1)}) %all-gather.13.cloned.1.call-update) | async-done | bytes 1048592 | tf_op jit(solution)/shard_map/all_gather | solution.py:43
  60.9 0.0 copy-done.4
  60.9 2.7 fusion.12
  63.6 26.2 %all-gather.11.cloned.1.call-done = bf16[2048,256]{1,0:T(8,128)(2,1)} async-done(((bf16[512,256]{1,0:T(8,128)(2,1)}), bf16[2048,256]{1,0:T(8,128)(2,1)}) %all-gather.11.cloned.1.call-update) | async-done | bytes 1048592 | tf_op jit(solution)/shard_map/all_gather | solution.py:42
  89.8 0.0 copy-done.1
  89.8 2.2 fusion.15
  92.1 1.6 fusion.76
  93.7 6.1 %all-reduce.1 = (f32[384]{0:T(512)S(1)}, f32[384]{0:T(512)S(1)}) all-reduce(f32[384]{0:T(512)S(1)} %get-tuple-element.6, f32[384]{0:T(512)S(1)} %get-tuple-element.5), channel_id=1, replica_groups=mesh['grp'=2,'fs'=4,'tp'=4] {'tp'}, use_global_device_ids=true, to_apply=%region_4.5 | all-reduce | flops 768 | bytes 6144 | tf_op jit(solution)/shard_map/psum | solution.py:53
  99.8 18.9 %all-gather.15.cloned.1.call-done = bf16[2048,256]{1,0:T(8,128)(2,1)} async-done(((bf16[512,256]{1,0:T(8,128)(2,1)}), bf16[2048,256]{1,0:T(8,128)(2,1)}) %all-gather.15.cloned.1.call-update) | async-done | bytes 1048592 | tf_op jit(solution)/shard_map/all_gather | solution.py:44
  118.6 0.0 copy-start.3
  118.7 3.1 fusion.8
  121.7 0.0 reduce-scatter.3.cloned.1.call-update
  121.8 0.0 all-gather.17.cloned.1.call-start
  121.8 0.0 copy-done.3
  121.8 0.2 copy.12
  122.0 27.2 %reduce-scatter.3.cloned.1.call-done = bf16[512,384]{0,1:T(8,128)(2,1)} async-done(((bf16[2048,384]{0,1:T(8,128)(2,1)}), bf16[512,384]{0,1:T(8,128)(2,1)}) %reduce-scatter.3.cloned.1.call-update) | async-done | bytes 393232 | tf_op jit(solution)/shard_map/reduce_scatter | solution.py:64
  149.3 1.8 add_convert_fusion.1
  151.1 0.0 all-gather.17.cloned.1.call-update
  151.1 0.0 all-gather.19.cloned.1.call-start
  151.2 0.7 all-gather.19.cloned.1.call-update
  151.9 0.0 copy-start.5
  151.9 0.0 all-gather.21.cloned.1.call-start
  151.9 0.7 all-gather.21.cloned.1.call-update
  152.7 0.0 all-gather.23.cloned.1.call-start
  152.7 0.7 all-gather.23.cloned.1.call-update
  153.4 0.0 reduce-scatter.5.cloned.1.call-start
  153.4 17.5 %all-gather.17.cloned.1.call-done = bf16[2048,384]{0,1:T(8,128)(2,1)} async-done(((bf16[512,384]{0,1:T(8,128)(2,1)}), bf16[2048,384]{0,1:T(8,128)(2,1)}) %all-gather.17.cloned.1.call-update) | async-done | bytes 1572880 | tf_op jit(solution)/shard_map/all_gather | solution.py:72
  170.9 1.8 fusion.3
  172.7 0.0 copy-start.2
  172.7 106.5 %all-gather.19.cloned.1.call-done = bf16[2048,1408]{1,0:T(8,128)(2,1)} async-done(((bf16[512,1408]{1,0:T(8,128)(2,1)}), bf16[2048,1408]{1,0:T(8,128)(2,1)}) %all-gather.19.cloned.1.call-update) | async-done | bytes 5767184 | tf_op jit(solution)/shard_map/all_gather | solution.py:75
  279.2 0.0 copy-done.5
  279.2 7.1 %convolution_bitcast_fusion.1 = f32[1408,384]{0,1:T(8,128)} fusion(bf16[2048,1408]{1,0:T(8,128)(2,1)} %all-gather.19.cloned.1.call-done, bf16[2048,384]{0,1:T(8,128)(2,1)} %all-gather.17.cloned.1.call-done, f32[2048]{0:T(1024)S(1)} %copy-done.5, f32[384]{0:T(512)S(1)} %add_rsqrt_fusion), kind=kOutput, calls=%fused_computation.12 | convolution fusion | flops 2217738240 | bytes 9512448 | tf_op jit(solution)/shard_map/dot_general | solution.py:13
  286.4 0.0 copy-start
  286.4 99.4 %all-gather.21.cloned.1.call-done = bf16[2048,1408]{1,0:T(8,128)(2,1)} async-done(((bf16[512,1408]{1,0:T(8,128)(2,1)}), bf16[2048,1408]{1,0:T(8,128)(2,1)}) %all-gather.21.cloned.1.call-update) | async-done | bytes 5767184 | tf_op jit(solution)/shard_map/all_gather | solution.py:76
  385.8 106.6 %all-gather.23.cloned.1.call-done = bf16[2048,1408]{1,0:T(8,128)(2,1)} async-done(((bf16[512,1408]{1,0:T(8,128)(2,1)}), bf16[2048,1408]{1,0:T(8,128)(2,1)}) %all-gather.23.cloned.1.call-update) | async-done | bytes 5767184 | tf_op jit(solution)/shard_map/all_gather | solution.py:81
  492.3 0.0 copy-done.2
  492.3 11.3 %fusion.9 = bf16[2048,384]{0,1:T(8,128)(2,1)} fusion(bf16[2048,1408]{1,0:T(8,128)(2,1)} %all-gather.23.cloned.1.call-done, bf16[2048,1408]{1,0:T(8,128)(2,1)} %all-gather.21.cloned.1.call-done, f32[1408,384]{0,1:T(8,128)} %convolution_bitcast_fusion.1, bf16[2048,384]{0,1:T(8,128)(2,1)S(1)} %copy-done.2, f32[2048]{0:T(1024)S(1)} %copy-done.5, ...), kind=kOutput, calls=%fused_computation.17 | convolution fusion | flops 4436361216 | bytes 16852480 | tf_op jit(solution)/shard_map/dot_general | solution.py:83
  503.6 0.0 reduce-scatter.5.cloned.1.call-update
  503.6 26.4 %reduce-scatter.5.cloned.1.call-done = bf16[512,384]{0,1:T(8,128)(2,1)} async-done(((bf16[2048,384]{0,1:T(8,128)(2,1)}), bf16[512,384]{0,1:T(8,128)(2,1)}) %reduce-scatter.5.cloned.1.call-update) | async-done | bytes 393232 | tf_op jit(solution)/shard_map/reduce_scatter | solution.py:82
  530.1 0.0 copy-done
  530.1 1.1 add_convert_fusion
  531.2 0.9 copy.13
  (5 shorter events, 0.1 us)
Async XLA Ops:
  6.5 54.3 %copy-start.4 = (f32[2048]{0:T(1024)S(1)}, f32[2048]{0:T(1024)}, u32[]{:S(2)}) copy-start(f32[2048]{0:T(1024)} %param.12) | copy-start | bytes 24580
  6.5 24.7 %all-gather.9.cloned.1.call-start = ((), (), s32[]{:S(2)}) async-start(), calls=%async_computation.2 | async-start | bytes 1966080 | tf_op jit(solution)/shard_map/all_gather | solution.py:39
  7.3 53.6 %all-gather.13.cloned.1.call-start = ((), (), s32[]{:S(2)}) async-start(), calls=%async_computation.4 | async-start | bytes 1310720 | tf_op jit(solution)/shard_map/all_gather | solution.py:43
  8.0 81.8 %all-gather.11.cloned.1.call-start = ((), (), s32[]{:S(2)}) async-start(), calls=%async_computation.3 | async-start | bytes 1310720 | tf_op jit(solution)/shard_map/all_gather | solution.py:42
  8.7 109.9 %all-gather.15.cloned.1.call-start = ((), (), s32[]{:S(2)}) async-start(), calls=%async_computation.5 | async-start | bytes 1310720 | tf_op jit(solution)/shard_map/all_gather | solution.py:44
  9.3 140.0 %reduce-scatter.3.cloned.1.call-start = ((), (), s32[]{:S(2)}) async-start(), calls=%async_computation.6 | async-start | bytes 1966080 | tf_op jit(solution)/shard_map/reduce_scatter | solution.py:64
  33.1 56.7 %copy-start.1 = (bf16[2048,384]{1,0:T(8,128)(2,1)S(1)}, bf16[2048,384]{1,0:T(8,128)(2,1)}, u32[]{:S(2)}) copy-start(bf16[2048,384]{1,0:T(8,128)(2,1)} %all-gather.9.cloned.1.call-done) | copy-start | bytes 4718596
  118.6 3.2 copy-start.3
  121.8 49.2 %all-gather.17.cloned.1.call-start = ((), (), s32[]{:S(2)}) async-start(), calls=%async_computation.7 | async-start | bytes 1966080 | tf_op jit(solution)/shard_map/all_gather | solution.py:72
  151.1 128.1 %all-gather.19.cloned.1.call-start = ((), (), s32[]{:S(2)}) async-start(), calls=%async_computation.8 | async-start | bytes 7208960 | tf_op jit(solution)/shard_map/all_gather | solution.py:75
  151.9 127.3 %copy-start.5 = (f32[2048]{0:T(1024)S(1)}, f32[2048]{0:T(1024)}, u32[]{:S(2)}) copy-start(f32[2048]{0:T(1024)} %param.18) | copy-start | bytes 24580
  151.9 233.9 %all-gather.21.cloned.1.call-start = ((), (), s32[]{:S(2)}) async-start(), calls=%async_computation.9 | async-start | bytes 7208960 | tf_op jit(solution)/shard_map/all_gather | solution.py:76
  152.7 339.7 %all-gather.23.cloned.1.call-start = ((), (), s32[]{:S(2)}) async-start(), calls=%async_computation.10 | async-start | bytes 7208960 | tf_op jit(solution)/shard_map/all_gather | solution.py:81
  153.4 376.7 %reduce-scatter.5.cloned.1.call-start = ((), (), s32[]{:S(2)}) async-start(), calls=%async_computation.11 | async-start | bytes 1966080 | tf_op jit(solution)/shard_map/reduce_scatter | solution.py:82
  172.7 319.6 %copy-start.2 = (bf16[2048,384]{0,1:T(8,128)(2,1)S(1)}, bf16[2048,384]{0,1:T(8,128)(2,1)}, u32[]{:S(2)}) copy-start(bf16[2048,384]{0,1:T(8,128)(2,1)} %all-gather.17.cloned.1.call-done) | copy-start | bytes 4718596
  286.4 243.7 %copy-start = (bf16[512,384]{0,1:T(8,128)(2,1)S(1)}, bf16[512,384]{0,1:T(8,128)(2,1)}, u32[]{:S(2)}) copy-start(bf16[512,384]{0,1:T(8,128)(2,1)} %add_convert_fusion.1) | copy-start | bytes 1179652
Sparse Core Ops, SparseCore 0:
  8.9 22.3 all-gather.8
  32.8 27.9 all-gather.12
  62.4 27.3 all-gather.10
  91.3 27.3 all-gather.14
  121.9 27.3 reduce-scatter.2
  151.3 19.6 all-gather.16
  172.5 106.6 all-gather.18
  280.8 104.9 all-gather.20
  387.4 104.9 all-gather.22
  503.8 26.2 reduce-scatter.4
where the time goes:
time: 539 us
  waiting for transfers between devices  482 us (89%)
  matrix products  26.5 us (5%)
  between operations  13.6 us (3%)
  other arithmetic  8.9 us (2%)
  blocking collectives  6.08 us (1%)
    all_gather x1, waiting for transfers between devices, on_device(): down_whole = lax.all_gather(ffn_down, 'fs', axis=0, tiled=True)  107 us
    all_gather x1, waiting for transfers between devices, on_device(): lax.all_gather(ffn_gate, 'fs', axis=0, tiled=True)  106 us
    all_gather x1, waiting for transfers between devices, on_device(): lax.all_gather(ffn_up, 'fs', axis=0, tiled=True)  99.4 us
    all_gather x1, waiting for transfers between devices, on_device(): lax.all_gather(glu_gate, 'fs', axis=0, tiled=True)  27.8 us
    reduce_scatter x1, waiting for transfers between devices, on_device(): lax.psum_scatter(jnp.dot(out_w, activated, preferred_element_type=jnp.flo...  27.2 us
    reduce_scatter x1, waiting for transfers between devices, on_device(): lax.psum_scatter(jnp.dot(down_whole, hidden, preferred_element_type=jnp.f...  26.4 us
    all_gather x1, waiting for transfers between devices, on_device(): lax.all_gather(glu_value, 'fs', axis=0, tiled=True)  26.2 us
    all_gather x1, waiting for transfers between devices, on_device(): gathered = lax.all_gather(stream, 'tp', axis=0, tiled=True)  20.4 us
  transfers between devices with their start and end apart: 10, of which 10 were waited for; matrix products, arithmetic and copies ran while one was open for 4% of the time, Pallas kernels for 0%

commit v1 on v0

--- a/solution.py
+++ b/solution.py
@@ -2,6 +2,20 @@
 import jax.numpy as jnp
 from jax import lax
 from jax.sharding import PartitionSpec as P
+from jax.lax import axis_index, axis_size, ppermute
+
+
+def view_cells_by_axis(x0, axis_id="fs"):
+    nd = axis_size(axis_id)
+    samples = tuple(((m, (m + 1) % nd) for m in range(nd)))
+    n_now = [None] * nd
+    n_now[nd - 1] = x0
+    for to_i in range(nd - 2, -1, -1):
+        n_now[to_i] = ppermute(n_now[to_i + 1], axis_id, samples)
+    block_now = jnp.roll(
+        jnp.concatenate(n_now, axis=0), (axis_index(axis_id) + 1) * x0.shape[0], axis=0
+    )
+    return block_now
 
 
 def rms_normalize(wide, gain):
@@ -78,7 +92,7 @@
     gate_val = contract(gate_whole, normed_two)
     up_val = contract(up_whole, normed_two)
     hidden = (jax.nn.silu(gate_val) * up_val).astype(jnp.bfloat16)
-    down_whole = lax.all_gather(ffn_down, "fs", axis=0, tiled=True)
+    down_whole = view_cells_by_axis(ffn_down)
     ffn_sum = lax.psum_scatter(
         jnp.dot(down_whole, hidden, preferred_element_type=jnp.float32).astype(jnp.bfloat16),
         "tp",

time: 539 us -> 498 us (0.924)
  waiting for transfers between devices: 482 us -> 386 us
  starting transfers between devices: 0.35 us -> 36.6 us
  local copies, waits for them, and re-layouts: 1.93 us -> 17.5 us
    ppermute x0 -> x3, waiting for transfers between devices: none -> 154 us  [view_cells_by_axis(): n_now[to_i] = ppermute(n_now[to_i + 1], axis_id, samples)]
    all_gather x1 -> x0, waiting for transfers between devices: 107 us -> none  [on_device(): down_whole = lax.all_gather(ffn_down, 'fs', axis=0, tiled=True)]
    all_gather x1, waiting for transfers between devices: 106 us -> 0.02 us  [on_device(): lax.all_gather(ffn_gate, 'fs', axis=0, tiled=True)]
    ppermute x0 -> x3, starting transfers between devices: none -> 36.3 us  [view_cells_by_axis(): n_now[to_i] = ppermute(n_now[to_i + 1], axis_id, samples)]
    all_gather x1, waiting for transfers between devices: 99.4 us -> 81.2 us  [on_device(): lax.all_gather(ffn_up, 'fs', axis=0, tiled=True)]
    all_gather x1, waiting for transfers between devices: 17.5 us -> 0.01 us  [on_device(): gathered_two = lax.all_gather(middle, 'tp', axis=0, tiled=True)]
    unnamed x13 -> x22, local copies, waits for them, and re-layouts: 0.21 us -> 14.4 us
    dot_general x3 -> x4, matrix products: 12.1 us -> 18.2 us  [contract(): lax.dot_general(weight, acts, (((0,), (0,)), ((), ())), preferred_element...]
  transfers between devices with their start and end apart: 10 -> 12, of which waited for: 10 -> 10; matrix products, arithmetic and copies ran while one was open for 4% -> 7% of each run, Pallas kernels for 0% -> 0%
where the time goes in v1:
time: 498 us; the launch traced here: 497 us
  waiting for transfers between devices  386 us (78%)
  starting transfers between devices  36.6 us (7%)
  matrix products  29 us (6%)
  local copies, waits for them, and re-layouts  17.5 us (4%)
  between operations  13.3 us (3%)
  other arithmetic  8.92 us (2%)
  blocking collectives  6.08 us (1%)
    ppermute x3, waiting for transfers between devices, view_cells_by_axis(): n_now[to_i] = ppermute(n_now[to_i + 1], axis_id, samples)  154 us
    all_gather x1, waiting for transfers between devices, on_device(): lax.all_gather(ffn_up, 'fs', axis=0, tiled=True)  81.2 us
    ppermute x3, starting transfers between devices, view_cells_by_axis(): n_now[to_i] = ppermute(n_now[to_i + 1], axis_id, samples)  36.3 us
    all_gather x1, waiting for transfers between devices, on_device(): lax.all_gather(glu_gate, 'fs', axis=0, tiled=True)  27.7 us
    reduce_scatter x1, waiting for transfers between devices, on_device(): lax.psum_scatter(jnp.dot(out_w, activated, preferred_element_type=jnp.flo...  27.3 us
    reduce_scatter x1, waiting for transfers between devices, on_device(): lax.psum_scatter(jnp.dot(down_whole, hidden, preferred_element_type=jnp.f...  26.5 us
    all_gather x1, waiting for transfers between devices, on_device(): lax.all_gather(glu_value, 'fs', axis=0, tiled=True)  26.2 us
    all_gather x1, waiting for transfers between devices, on_device(): gathered = lax.all_gather(stream, 'tp', axis=0, tiled=True)  20.4 us
  transfers between devices with their start and end apart: 12, of which 10 were waited for; matrix products, arithmetic and copies ran while one was open for 7% of the time, Pallas kernels for 0%

profile of v1, /device:TPU:0, one launch (start us, length us, event | category | flops | bytes accessed | tf_op | source)
XLA Modules:
  0.0 497.1 jit_solution(9108394686141437673)
XLA Ops:
  6.5 0.0 all-gather.8.cloned.1.call-start
  6.5 0.7 all-gather.8.cloned.1.call-update
  7.3 0.0 all-gather.12.cloned.1.call-start
  7.3 0.7 all-gather.12.cloned.1.call-update
  8.0 0.0 all-gather.10.cloned.1.call-start
  8.1 0.7 all-gather.10.cloned.1.call-update
  8.7 0.0 all-gather.14.cloned.1.call-start
  8.8 0.5 all-gather.14.cloned.1.call-update
  9.3 0.0 reduce-scatter.3.cloned.1.call-start
  9.4 0.7 dynamic-slice_convert_fusion
  10.1 0.8 dynamic_slice.11
  10.9 20.4 %all-gather.8.cloned.1.call-done = bf16[2048,384]{1,0:T(8,128)(2,1)} async-done(((bf16[512,384]{1,0:T(8,128)(2,1)}), bf16[2048,384]{1,0:T(8,128)(2,1)}) %all-gather.8.cloned.1.call-update) | async-done | bytes 1572880 | tf_op jit(solution)/shard_map/all_gather | solution.py:53
  31.3 1.8 fusion.2
  33.1 0.0 copy-start.5
  33.1 27.7 %all-gather.12.cloned.1.call-done = bf16[2048,256]{1,0:T(8,128)(2,1)} async-done(((bf16[512,256]{1,0:T(8,128)(2,1)}), bf16[2048,256]{1,0:T(8,128)(2,1)}) %all-gather.12.cloned.1.call-update) | async-done | bytes 1048592 | tf_op jit(solution)/shard_map/all_gather | solution.py:57
  60.9 2.7 fusion.16
  63.6 26.2 %all-gather.10.cloned.1.call-done = bf16[2048,256]{1,0:T(8,128)(2,1)} async-done(((bf16[512,256]{1,0:T(8,128)(2,1)}), bf16[2048,256]{1,0:T(8,128)(2,1)}) %all-gather.10.cloned.1.call-update) | async-done | bytes 1048592 | tf_op jit(solution)/shard_map/all_gather | solution.py:56
  89.8 0.0 copy-done.3
  89.8 0.0 copy-done.5
  89.8 2.2 fusion.19
  92.1 0.0 copy-start.4
  92.1 1.6 fusion.79
  93.7 6.1 %all-reduce.1 = (f32[384]{0:T(512)S(1)}, f32[384]{0:T(512)S(1)}) all-reduce(f32[384]{0:T(512)S(1)} %get-tuple-element.6, f32[384]{0:T(512)S(1)} %get-tuple-element.5), channel_id=1, replica_groups=mesh['grp'=2,'fs'=4,'tp'=4] {'tp'}, use_global_device_ids=true, to_apply=%region_4.5 | all-reduce | flops 768 | bytes 6144 | tf_op jit(solution)/shard_map/psum | solution.py:67
  99.8 18.9 %all-gather.14.cloned.1.call-done = bf16[2048,256]{1,0:T(8,128)(2,1)} async-done(((bf16[512,256]{1,0:T(8,128)(2,1)}), bf16[2048,256]{1,0:T(8,128)(2,1)}) %all-gather.14.cloned.1.call-update) | async-done | bytes 1048592 | tf_op jit(solution)/shard_map/all_gather | solution.py:58
  118.6 3.0 fusion.13
  121.7 0.0 reduce-scatter.3.cloned.1.call-update
  121.7 0.0 all-gather.16.cloned.1.call-start
  121.8 0.0 copy-done.4
  121.8 0.2 copy.12
  122.0 27.3 %reduce-scatter.3.cloned.1.call-done = bf16[512,384]{0,1:T(8,128)(2,1)} async-done(((bf16[2048,384]{0,1:T(8,128)(2,1)}), bf16[512,384]{0,1:T(8,128)(2,1)}) %reduce-scatter.3.cloned.1.call-update) | async-done | bytes 393232 | tf_op jit(solution)/shard_map/reduce_scatter | solution.py:78
  149.2 1.8 add_convert_fusion.1
  151.1 0.0 all-gather.16.cloned.1.call-update
  151.1 0.0 all-gather.18.cloned.1.call-start
  151.2 0.7 all-gather.18.cloned.1.call-update
  151.9 0.0 all-gather.20.cloned.1.call-start
  151.9 0.7 all-gather.20.cloned.1.call-update
  152.6 0.0 reduce-scatter.5.cloned.1.call-start
  152.7 0.0 copy-done
  152.7 1.5 collective-permute-start
  154.2 36.8 %collective-permute-done = bf16[512,1408]{1,0:T(8,128)(2,1)S(1)} collective-permute-done((bf16[512,1408]{1,0:T(8,128)(2,1)S(1)}, bf16[512,1408]{1,0:T(8,128)(2,1)S(1)}, u32[]{:S(2)}, u32[]{:S(2)}) %collective-permute-start) | collective-permute-done | bytes 1441824 | tf_op jit(solution)/shard_map/ppermute | solution.py:14
  191.0 3.6 collective-permute-start.1
  194.6 64.4 %collective-permute-done.1 = bf16[512,1408]{1,0:T(8,128)(2,1)} collective-permute-done((bf16[512,1408]{1,0:T(8,128)(2,1)S(1)}, bf16[512,1408]{1,0:T(8,128)(2,1)}, u32[]{:S(2)}, u32[]{:S(2)}) %collective-permute-start.1) | collective-permute-done | bytes 1441824 | tf_op jit(solution)/shard_map/ppermute | solution.py:14
  259.0 31.2 %collective-permute-start.2 = (bf16[512,1408]{1,0:T(8,128)(2,1)}, bf16[512,1408]{1,0:T(8,128)(2,1)}, u32[]{:S(2)}, u32[]{:S(2)}) collective-permute-start(bf16[512,1408]{1,0:T(8,128)(2,1)} %collective-permute-done.1), channel_id=1, source_target_pairs={{0,4},{4,8},{8,12},{12,0},{1,5},{5,9},{9,13},{13,1},{2,6},{6,10},{... | collective-permute-start | bytes 4325384 | tf_op jit(solution)/shard_map/ppermute | solution.py:14
  290.1 52.3 %collective-permute-done.2 = bf16[512,1408]{1,0:T(8,128)(2,1)} collective-permute-done((bf16[512,1408]{1,0:T(8,128)(2,1)}, bf16[512,1408]{1,0:T(8,128)(2,1)}, u32[]{:S(2)}, u32[]{:S(2)}) %collective-permute-start.2) | collective-permute-done | bytes 1441824 | tf_op jit(solution)/shard_map/ppermute | solution.py:14
  342.5 2.6 constant_dynamic-update-slice_fusion.7
  345.1 2.6 constant_dynamic-update-slice_fusion.6
  347.6 1.2 constant_dynamic-update-slice_fusion.5
  348.9 1.2 constant_dynamic-update-slice_fusion.4
  350.1 2.8 constant_dynamic-update-slice_fusion.3
  352.9 2.6 constant_dynamic-update-slice_fusion.2
  355.5 1.2 constant_dynamic-update-slice_fusion.1
  356.7 1.3 constant_dynamic-update-slice_fusion
  358.0 1.8 fusion.5
  359.8 0.0 all-gather.18.cloned.1.call-done
  359.9 7.3 %convolution_bitcast_fusion.1 = f32[1408,384]{0,1:T(8,128)} fusion(bf16[2048,1408]{1,0:T(8,128)(2,1)} %all-gather.18.cloned.1.call-done, bf16[2048,384]{0,1:T(8,128)(2,1)} %all-gather.16.cloned.1.call-done, f32[2048]{0:T(1024)S(1)} %copy-done.6, f32[384]{0:T(512)S(1)} %add_rsqrt_fusion), kind=kOutput, calls=%fused_computation.14 | convolution fusion | flops 2217738240 | bytes 9512448 | tf_op jit(solution)/shard_map/dot_general | solution.py:27
  367.1 81.2 %all-gather.20.cloned.1.call-done = bf16[2048,1408]{1,0:T(8,128)(2,1)} async-done(((bf16[512,1408]{1,0:T(8,128)(2,1)}), bf16[2048,1408]{1,0:T(8,128)(2,1)}) %all-gather.20.cloned.1.call-update) | async-done | bytes 5767184 | tf_op jit(solution)/shard_map/all_gather | solution.py:90
  448.3 6.0 %fusion.9 = bf16[1408,384]{0,1:T(8,128)(2,1)S(1)} fusion(bf16[2048,1408]{1,0:T(8,128)(2,1)} %all-gather.20.cloned.1.call-done, f32[1408,384]{0,1:T(8,128)} %convolution_bitcast_fusion.1, bf16[2048,384]{0,1:T(8,128)(2,1)S(1)} %copy-done.2, f32[2048]{0:T(1024)S(1)} %copy-done.6, f32[384]{0:T(512)S(1)} %add_rsqrt_fusion), kind=kOutput, calls=%fused_computation.15 | convolution fusion | flops 2220982272 | bytes 10593792 | tf_op jit(solution)/shard_map/dot_general | solution.py:27
  454.2 0.0 copy-start.1
  454.3 7.7 %fusion.10 = bf16[2048,384]{0,1:T(8,128)(2,1)} fusion(bf16[1408,384]{0,1:T(8,128)(2,1)S(1)} %fusion.9, bf16[4096,1408]{1,0:T(8,128)(2,1)} %constant_dynamic-update-slice_fusion, s32[]{:T(128)S(6)} %select_n.19), kind=kOutput, calls=%fused_computation.16 | convolution fusion | flops 2215378944 | bytes 8421380 | tf_op jit(solution)/shard_map/dot_general | solution.py:97
  462.0 0.0 reduce-scatter.5.cloned.1.call-update
  462.0 26.5 %reduce-scatter.5.cloned.1.call-done = bf16[512,384]{0,1:T(8,128)(2,1)} async-done(((bf16[2048,384]{0,1:T(8,128)(2,1)}), bf16[512,384]{0,1:T(8,128)(2,1)}) %reduce-scatter.5.cloned.1.call-update) | async-done | bytes 393232 | tf_op jit(solution)/shard_map/reduce_scatter | solution.py:96
  488.5 0.0 copy-done.1
  488.5 1.1 add_convert_fusion
  489.6 0.9 copy.14
  (12 shorter events, 0.1 us)
Async XLA Ops:
  6.5 24.7 %all-gather.8.cloned.1.call-start = ((), (), s32[]{:S(2)}) async-start(), calls=%async_computation.2 | async-start | bytes 1966080 | tf_op jit(solution)/shard_map/all_gather | solution.py:53
  7.3 53.6 %all-gather.12.cloned.1.call-start = ((), (), s32[]{:S(2)}) async-start(), calls=%async_computation.4 | async-start | bytes 1310720 | tf_op jit(solution)/shard_map/all_gather | solution.py:57
  8.0 81.8 %all-gather.10.cloned.1.call-start = ((), (), s32[]{:S(2)}) async-start(), calls=%async_computation.3 | async-start | bytes 1310720 | tf_op jit(solution)/shard_map/all_gather | solution.py:56
  8.7 109.9 %all-gather.14.cloned.1.call-start = ((), (), s32[]{:S(2)}) async-start(), calls=%async_computation.5 | async-start | bytes 1310720 | tf_op jit(solution)/shard_map/all_gather | solution.py:58
  9.3 139.9 %reduce-scatter.3.cloned.1.call-start = ((), (), s32[]{:S(2)}) async-start(), calls=%async_computation.6 | async-start | bytes 1966080 | tf_op jit(solution)/shard_map/reduce_scatter | solution.py:78
  33.1 56.7 %copy-start.3 = (bf16[2048,384]{1,0:T(8,128)(2,1)S(1)}, bf16[2048,384]{1,0:T(8,128)(2,1)}, u32[]{:S(2)}) copy-start(bf16[2048,384]{1,0:T(8,128)(2,1)} %all-gather.8.cloned.1.call-done) | copy-start | bytes 4718596
  33.1 56.7 %copy-start.5 = (f32[2048]{0:T(1024)S(1)}, f32[2048]{0:T(1024)}, u32[]{:S(2)}) copy-start(f32[2048]{0:T(1024)} %param.12) | copy-start | bytes 24580
  92.1 29.7 %copy-start.4 = (bf16[512,384]{1,0:T(8,128)(2,1)S(1)}, bf16[512,384]{1,0:T(8,128)(2,1)}, u32[]{:S(2)}) copy-start(bf16[512,384]{1,0:T(8,128)(2,1)} %param.11) | copy-start | bytes 1179652
  121.7 31.0 %copy-start = (bf16[512,1408]{1,0:T(8,128)(2,1)S(1)}, bf16[512,1408]{1,0:T(8,128)(2,1)}, u32[]{:S(2)}) copy-start(bf16[512,1408]{1,0:T(8,128)(2,1)} %param.21) | copy-start | bytes 4325380
  121.7 236.3 %all-gather.16.cloned.1.call-start = ((), (), s32[]{:S(2)}) async-start(), calls=%async_computation.7 | async-start | bytes 1966080 | tf_op jit(solution)/shard_map/all_gather | solution.py:86
  151.1 208.7 %all-gather.18.cloned.1.call-start = ((), (), s32[]{:S(2)}) async-start(), calls=%async_computation.8 | async-start | bytes 7208960 | tf_op jit(solution)/shard_map/all_gather | solution.py:89
  151.9 296.4 %all-gather.20.cloned.1.call-start = ((), (), s32[]{:S(2)}) async-start(), calls=%async_computation.9 | async-start | bytes 7208960 | tf_op jit(solution)/shard_map/all_gather | solution.py:90
  152.6 335.9 %reduce-scatter.5.cloned.1.call-start = ((), (), s32[]{:S(2)}) async-start(), calls=%async_computation.10 | async-start | bytes 1966080 | tf_op jit(solution)/shard_map/reduce_scatter | solution.py:96
  152.7 38.3 %collective-permute-start = (bf16[512,1408]{1,0:T(8,128)(2,1)S(1)}, bf16[512,1408]{1,0:T(8,128)(2,1)S(1)}, u32[]{:S(2)}, u32[]{:S(2)}) collective-permute-start(bf16[512,1408]{1,0:T(8,128)(2,1)S(1)} %copy-done), channel_id=1, source_target_pairs={{0,4},{4,8},{8,12},{12,0},{1,5},{5,9},{9,13},{13,1},{2,6},{6,10},{... | collective-permute-start | bytes 4325384 | tf_op jit(solution)/shard_map/ppermute | solution.py:14
  191.0 68.0 %collective-permute-start.1 = (bf16[512,1408]{1,0:T(8,128)(2,1)S(1)}, bf16[512,1408]{1,0:T(8,128)(2,1)}, u32[]{:S(2)}, u32[]{:S(2)}) collective-permute-start(bf16[512,1408]{1,0:T(8,128)(2,1)S(1)} %collective-permute-done), channel_id=1, source_target_pairs={{0,4},{4,8},{8,12},{12,0},{1,5},{5,9},{9,13},{13,1},{2,6},{6,10},{... | collective-permute-start | bytes 4325384 | tf_op jit(solution)/shard_map/ppermute | solution.py:14
  259.0 83.5 %collective-permute-start.2 = (bf16[512,1408]{1,0:T(8,128)(2,1)}, bf16[512,1408]{1,0:T(8,128)(2,1)}, u32[]{:S(2)}, u32[]{:S(2)}) collective-permute-start(bf16[512,1408]{1,0:T(8,128)(2,1)} %collective-permute-done.1), channel_id=1, source_target_pairs={{0,4},{4,8},{8,12},{12,0},{1,5},{5,9},{9,13},{13,1},{2,6},{6,10},{... | collective-permute-start | bytes 4325384 | tf_op jit(solution)/shard_map/ppermute | solution.py:14
  355.5 4.4 copy-start.6
  359.8 88.5 %copy-start.2 = (bf16[2048,384]{0,1:T(8,128)(2,1)S(1)}, bf16[2048,384]{0,1:T(8,128)(2,1)}, u32[]{:S(2)}) copy-start(bf16[2048,384]{0,1:T(8,128)(2,1)} %all-gather.16.cloned.1.call-done) | copy-start | bytes 4718596
  454.2 34.3 %copy-start.1 = (bf16[512,384]{0,1:T(8,128)(2,1)S(1)}, bf16[512,384]{0,1:T(8,128)(2,1)}, u32[]{:S(2)}) copy-start(bf16[512,384]{0,1:T(8,128)(2,1)} %add_convert_fusion.1) | copy-start | bytes 1179652
Sparse Core Ops, SparseCore 0:
  8.9 22.3 all-gather.7
  32.8 27.9 all-gather.11
  62.4 27.3 all-gather.9
  91.3 27.3 all-gather.13
  121.8 27.3 reduce-scatter.2
  151.2 19.6 all-gather.15
  172.5 170.2 all-gather.17
  344.3 103.9 all-gather.19
  462.2 26.3 reduce-scatter.4
